TPU v7x, 32 devices: a whole 2x2x4 slice. The times are simulated.
32 devices in a mesh: kv: 8 (over z, y), tp: 4 (over x, core).
Axes of the slice: x: 2, y: 2, z: 4, core: 2. Of those that a mesh axis runs over, the one named last changes fastest.
Arguments:
- tokens: bfloat16 [64, 4096], P(None, 'kv'), may hold values from -8 to 8
- attn_gain: float32 [4096], P('kv'), may hold values from 0.1 to 1.9
- w_query: bfloat16 [4096, 2048], P('kv', 'tp'), may hold values from -0.09375 to 0.09375
- w_key: bfloat16 [4096, 2048], P('kv', 'tp'), may hold values from -0.09375 to 0.09375
- w_value: bfloat16 [4096, 4096], P('kv', 'tp'), may hold values from -0.09375 to 0.09375
- w_outgate: bfloat16 [4096, 4096], P('kv', 'tp'), may hold values from -0.09375 to 0.09375
- w_gates: bfloat16 [4096, 16], replicated, may hold values from -0.029907227 to 0.029907227
- forget_bias: float32 [8], replicated, may hold values from -1 to 3
- state_c: float32 [64, 8, 512, 256], P('kv', 'tp'), may hold values from -6 to 6
- state_n: float32 [64, 8, 256], P('kv', 'tp'), may hold values from -6 to 6
- state_m: float32 [64, 8], P('kv', 'tp'), may hold values from -2 to 0.5
- w_output: bfloat16 [4096, 4096], P('tp', 'kv'), may hold values from -0.09375 to 0.09375
- mlp_gain: float32 [4096], P('kv'), may hold values from 0.1 to 1.9
- w_gateff: bfloat16 [4096, 11008], P('kv', 'tp'), may hold values from -0.09375 to 0.09375
- w_upff: bfloat16 [4096, 11008], P('kv', 'tp'), may hold values from -0.09375 to 0.09375
- w_downff: bfloat16 [11008, 4096], P('tp', 'kv'), may hold values from -0.0546875 to 0.0546875
Outputs:
- mixed: bfloat16 [64, 4096], P(None, 'kv')
- new_c: float32 [64, 8, 512, 256], P('kv', 'tp')
- new_n: float32 [64, 8, 256], P('kv', 'tp')
- new_m: float32 [64, 8], P('kv', 'tp')
All inputs are finite; a program needn't handle non-finite values.
Results may differ from a plain program's by a relative error of at most 0.0083.
Values may be sent and summed in bfloat16 or wider, within the bound.
A program may use at most 64 MiB of HBM per device.

v0:
```python
import jax
import jax.numpy as jnp
from jax import lax
from jax.sharding import PartitionSpec as P

norm_floor = 1e-05


def per_device(
    tokens,
    attn_gain,
    w_query,
    w_key,
    w_value,
    w_outgate,
    w_gates,
    forget_bias,
    state_c,
    state_n,
    state_m,
    w_output,
    mlp_gain,
    w_gateff,
    w_upff,
    w_downff,
):
    kv_count = lax.axis_size("kv")
    kv_at = lax.axis_index("kv")
    tp_at = lax.axis_index("tp")
    batch = tokens.shape[0]
    width_dev = tokens.shape[1]
    width_all = width_dev * kv_count
    rows = batch // kv_count
    heads_dev = state_c.shape[1]
    heads_all = forget_bias.shape[0]
    value_size = state_c.shape[2]
    query_size = state_c.shape[3]
    tok_float = tokens.astype(jnp.float32)
    squares_one = jnp.sum(tok_float * tok_float, axis=1)
    normed_one = (tok_float * attn_gain).astype(jnp.bfloat16)
    total_one = lax.psum(squares_one, "kv")
    rows_one = lax.dynamic_slice_in_dim(total_one, kv_at * rows, rows, 0)
    query_width = heads_dev * query_size
    value_width = heads_dev * value_size
    stacked = jnp.concatenate([w_query, w_key, w_value, w_outgate], axis=1)
    proj_part = jnp.dot(normed_one, stacked, preferred_element_type=jnp.float32)
    gate_rows = lax.dynamic_slice_in_dim(w_gates, kv_at * width_dev, width_dev, 0)
    gate_part = jnp.dot(normed_one, gate_rows, preferred_element_type=jnp.float32)
    extra_one = ()
    summed_one = lax.psum_scatter(
        (proj_part, gate_part) + extra_one, "kv", scatter_dimension=0, tiled=True
    )
    scale_one = lax.rsqrt(rows_one / width_all + norm_floor)[:, None]
    proj_rows = summed_one[0] * scale_one
    gate_all = summed_one[1] * scale_one
    query = (proj_rows[:, :query_width] * query_size ** (-0.5)).reshape(rows, heads_dev, query_size)
    key_vec = proj_rows[:, query_width : 2 * query_width].reshape(rows, heads_dev, query_size)
    value = proj_rows[:, 2 * query_width : 2 * query_width + value_width].reshape(
        rows, heads_dev, value_size
    )
    out_pre = proj_rows[:, 2 * query_width + value_width :].reshape(rows, heads_dev, value_size)
    log_input = lax.dynamic_slice_in_dim(gate_all, tp_at * heads_dev, heads_dev, 1)
    forget_pre = lax.dynamic_slice_in_dim(gate_all, heads_all + tp_at * heads_dev, heads_dev, 1)
    bias_dev = lax.dynamic_slice_in_dim(forget_bias, tp_at * heads_dev, heads_dev, 0)
    log_forget = jax.nn.log_sigmoid(forget_pre + bias_dev)
    carried = log_forget + state_m
    new_m = jnp.maximum(carried, log_input)
    keep = jnp.exp(carried - new_m)
    admit = jnp.exp(log_input - new_m)
    new_c = (
        keep[:, :, None, None] * state_c
        + admit[:, :, None, None] * value[:, :, :, None] * key_vec[:, :, None, :]
    )
    new_n = keep[:, :, None] * state_n + admit[:, :, None] * key_vec
    numer = jnp.einsum("bhvd,bhd->bhv", new_c, query, precision=lax.Precision.HIGHEST)
    denom = jnp.maximum(jnp.abs(jnp.sum(new_n * query, axis=-1)), jnp.exp(-new_m))
    head_out = (
        (jax.nn.sigmoid(out_pre) * numer / denom[:, :, None])
        .reshape(rows, value_width)
        .astype(jnp.bfloat16)
    )
    attn_part = jnp.dot(
        lax.all_gather(head_out, "kv", axis=0, tiled=True),
        w_output,
        preferred_element_type=jnp.float32,
    )
    attn_mix = lax.psum(attn_part, "tp")
    middle = (tok_float + attn_mix).astype(jnp.bfloat16)
    mid_float = middle.astype(jnp.float32)
    squares_two = jnp.sum(mid_float * mid_float, axis=1)
    normed_two = (mid_float * mlp_gain).astype(jnp.bfloat16)
    total_two = lax.psum(squares_two, "kv")
    gate_ff = jnp.dot(normed_two, w_gateff, preferred_element_type=jnp.float32)
    up_ff = jnp.dot(normed_two, w_upff, preferred_element_type=jnp.float32)
    extra_two = ()
    summed_two = lax.psum((gate_ff, up_ff) + extra_two, "kv")
    scale_two = lax.rsqrt(total_two / width_all + norm_floor)[:, None]
    hidden_ff = (jax.nn.silu(summed_two[0] * scale_two) * (summed_two[1] * scale_two)).astype(
        jnp.bfloat16
    )
    down_part = jnp.dot(hidden_ff, w_downff, preferred_element_type=jnp.float32)
    down_sum = lax.psum(down_part, "tp")
    mixed = (mid_float + down_sum).astype(jnp.bfloat16)
    return (mixed, new_c, new_n, new_m)


def solution(mesh):
    placed = (
        P(None, "kv"),
        P("kv"),
        P("kv", "tp"),
        P("kv", "tp"),
        P("kv", "tp"),
        P("kv", "tp"),
        P(),
        P(),
        P("kv", "tp", None, None),
        P("kv", "tp", None),
        P("kv", "tp"),
        P("tp", "kv"),
        P("kv"),
        P("kv", "tp"),
        P("kv", "tp"),
        P("tp", "kv"),
    )
    return jax.shard_map(
        per_device,
        mesh=mesh,
        in_specs=placed,
        out_specs=(P(None, "kv"), P("kv", "tp", None, None), P("kv", "tp", None), P("kv", "tp")),
        check_vma=False,
    )
```

profile of v0, /device:TPU:1, one launch (start us, length us, event | category | flops | bytes accessed | tf_op | source)
XLA Modules:
  0.0 291.7 jit_solution(13475774226316397294)
XLA Ops:
  7.2 0.0 copy-start
  7.2 0.0 copy-start.9
  7.2 0.0 copy-start.3
  7.2 0.0 copy-start.6
  7.2 0.0 reduce-scatter.2.cloned.1.call-start
  7.3 3.6 %fusion = f32[64,3072]{1,0:T(8,128)} fusion(bf16[512,1024]{1,0:T(8,128)(2,1)} %param.21, bf16[512,1024]{1,0:T(8,128)(2,1)} %param.20, bf16[512,512]{1,0:T(8,128)(2,1)} %param.19, bf16[512,512]{1,0:T(8,128)(2,1)} %param.18, bf16[64,512]{1,0:T(8,128)(2,1)} %param.16, f32[512]{0:T(512)} %param.17), kind=kOutput, calls=%fused_computation.1 | convolution fusion | flops 214007808 | bytes 3999744 | tf_op jit(solution)/shard_map/dot_general | solution.py:46
  10.8 0.0 reduce-scatter.2.cloned.1.call-update
  10.9 0.0 all-reduce.7.cloned.1.call-start
  10.9 0.1 copy.28
  11.0 0.6 dynamic-slice
  12.3 0.1 dynamic_slice.18
  12.4 0.1 fusion.12
  12.5 0.9 fusion.21
  13.3 31.5 %all-reduce.1 = (f32[64]{0:T(128)S(1)}, f32[64,16]{1,0:T(8,128)S(1)}) all-reduce(f32[64]{0:T(128)S(1)} %fusion.12, f32[64,16]{1,0:T(8,128)S(1)} %fusion.21), channel_id=1, replica_groups=mesh['kv'=8,'tp'=4] {'kv'}, use_global_device_ids=true, to_apply=%region_2.0 | all-reduce | flops 1088 | bytes 8704 | tf_op jit(solution)/shard_map/psum | solution.py:41
  44.8 0.1 add_rsqrt_fusion.1
  44.9 0.1 dynamic-slice_multiply_fusion
  45.0 0.1 subtract_exponential_fusion.1
  45.1 0.1 subtract_exponential_fusion
  45.2 0.1 copy.29
  45.3 30.2 %reduce-scatter.2.cloned.1.call-done = f32[8,3072]{1,0:T(8,128)} async-done(((f32[64,3072]{1,0:T(8,128)}), f32[8,3072]{1,0:T(8,128)}) %reduce-scatter.2.cloned.1.call-update) | async-done | bytes 98320 | tf_op jit(solution)/shard_map/reduce_scatter | solution.py:50
  75.4 1.0 broadcast_multiply_fusion
  76.4 0.1 broadcast_multiply_fusion.1
  76.5 0.7 fusion.31
  77.2 0.1 copy.34
  77.3 4.6 %multiply_add_fusion = f32[8,2,512,256]{3,2,1,0:T(8,128)S(1)} fusion(f32[8,2,512,256]{3,2,1,0:T(8,128)} %param.24, f32[8,2,256]{2,1,0:T(2,128)S(1)} %get-tuple-element.26, f32[8,2,512]{2,1,0:T(2,128)S(1)} %copy.30, f32[8,2]{1,0:T(8,128)S(1)} %get-tuple-element.20), kind=kLoop, calls=%fused_computation | loop fusion | flops 6291456 | bytes 16826432 | tf_op jit(solution)/shard_map/add | solution.py:71
  82.0 0.0 copy-start.1
  82.0 0.0 copy-start.2
  82.0 0.0 copy-start.5
  82.0 3.4 %copy-done.1 = f32[8,2,512,256]{3,2,1,0:T(8,128)} copy-done((f32[8,2,512,256]{3,2,1,0:T(8,128)}, f32[8,2,512,256]{3,2,1,0:T(8,128)S(1)}, u32[]{:S(2)}) %copy-start.1) | copy-done | bytes 8388632
  85.4 7.2 %fusion.29 = f32[8,2,1,512]{3,2,1,0:T(1,128)S(1)} fusion(f32[8,2,512,256]{3,2,1,0:T(8,128)S(1)} %multiply_add_fusion, f32[8,2,256,1]{2,0,1,3:T(8,128)S(1)} %bitcast.21), kind=kOutput, calls=%fused_computation.37 | convolution fusion | flops 25165824 | bytes 8437760 | tf_op jit(solution)/shard_map/bhvd,bhd->bhv/dot_general | solution.py:75
  92.5 0.1 fusion.28
  92.6 24.2 %all_gather.3 = bf16[64,1024]{1,0:T(8,128)(2,1)S(1)} all-gather(bf16[8,1024]{1,0:T(8,128)(2,1)S(1)} %bitcast.24), channel_id=1, replica_groups=mesh['kv'=8,'tp'=4] {'kv'}, dimensions={0}, use_global_device_ids=true | all-gather | bytes 147456 | tf_op jit(solution)/shard_map/all_gather | solution.py:83
  116.8 0.9 fusion.40
  117.8 0.0 all-reduce.7.cloned.1.call-update
  117.8 0.0 all-reduce.11.cloned.1.call-start
  117.9 37.5 %all-reduce.7.cloned.1.call-done = f32[64,512]{1,0:T(8,128)} async-done(((f32[64,512]{1,0:T(8,128)}), f32[64,512]{1,0:T(8,128)}) %all-reduce.7.cloned.1.call-update) | async-done | bytes 131088 | tf_op jit(solution)/shard_map/psum | solution.py:87
  155.4 1.0 fusion.15
  156.4 1.8 fusion.17
  158.3 3.6 %fusion.19 = f32[64,2752]{1,0:T(8,128)} fusion(bf16[512,2752]{0,1:T(8,128)(2,1)} %param.29, bf16[64,512]{1,0:T(8,128)(2,1)S(1)} %get-tuple-element.17, f32[512]{0:T(512)S(1)} %copy-done.5), kind=kOutput, calls=%fused_computation.26 | convolution fusion | flops 180453376 | bytes 3590144 | tf_op jit(solution)/shard_map/dot_general | solution.py:93
  161.9 0.0 all-reduce.11.cloned.1.call-update
  162.0 0.0 all-reduce.9.cloned.1.call-start
  162.0 18.6 %psum.45 = f32[64]{0:T(128)S(1)} all-reduce(f32[64]{0:T(128)S(1)} %get-tuple-element.16), channel_id=1, replica_groups=mesh['kv'=8,'tp'=4] {'kv'}, use_global_device_ids=true, to_apply=%region_8.9 | all-reduce | flops 64 | bytes 512 | tf_op jit(solution)/shard_map/psum | solution.py:92
  180.6 70.0 %all-reduce.11.cloned.1.call-done = (f32[64,2752]{1,0:T(8,128)}, f32[64,2752]{1,0:T(8,128)}) async-done(((f32[64,2752]{1,0:T(8,128)}, f32[64,2752]{1,0:T(8,128)}), (f32[64,2752]{1,0:T(8,128)}, f32[64,2752]{1,0:T(8,128)})) %all-reduce.11.cloned.1.call-update) | async-done | bytes 1409040 | tf_op jit(solution)/shard_map/psum | solution.py:96
  250.6 3.5 %fusion.8 = f32[64,512]{1,0:T(8,128)} fusion(bf16[2752,512]{1,0:T(8,128)(2,1)} %param.31, f32[64,2752]{1,0:T(8,128)} %get-tuple-element.14, f32[64,2752]{1,0:T(8,128)} %get-tuple-element.15, f32[64]{0:T(128)S(1)} %add_rsqrt_fusion), kind=kOutput, calls=%fused_computation.10 | convolution fusion | flops 181764096 | bytes 4358400 | tf_op jit(solution)/shard_map/dot_general | solution.py:101
  254.1 0.0 all-reduce.9.cloned.1.call-update
  254.1 0.6 copy.35
  254.8 28.8 %all-reduce.9.cloned.1.call-done = f32[64,512]{1,0:T(8,128)} async-done(((f32[64,512]{1,0:T(8,128)}), f32[64,512]{1,0:T(8,128)}) %all-reduce.9.cloned.1.call-update) | async-done | bytes 131088 | tf_op jit(solution)/shard_map/psum | solution.py:102
  283.6 1.5 fusion.16
  (17 shorter events, 0.1 us)
Async XLA Ops:
  7.2 149.3 %copy-start = (bf16[512,2752]{0,1:T(8,128)(2,1)S(1)}, bf16[512,2752]{0,1:T(8,128)(2,1)}, u32[]{:S(2)}) copy-start(bf16[512,2752]{0,1:T(8,128)(2,1)} %param.30) | copy-start | bytes 8454148
  7.2 3.8 %copy-start.9 = (u32[32]{0:T(128)S(1)}, u32[32]{0:T(128)}, u32[]{:S(2)}) copy-start(u32[32]{0:T(128)} %constant.49) | copy-start | bytes 388
  7.2 5.2 %copy-start.3 = (bf16[64,512]{1,0:T(8,128)(2,1)S(1)}, bf16[64,512]{1,0:T(8,128)(2,1)}, u32[]{:S(2)}) copy-start(bf16[64,512]{1,0:T(8,128)(2,1)} %param.16) | copy-start | bytes 196612
  7.2 5.3 %copy-start.6 = (f32[512]{0:T(512)S(1)}, f32[512]{0:T(512)}, u32[]{:S(2)}) copy-start(f32[512]{0:T(512)} %param.17) | copy-start | bytes 6148
  7.2 3.7 %copy-start.7 = (f32[8,2]{0,1:T(2,128)S(1)}, f32[8,2]{0,1:T(2,128)}, u32[]{:S(2)}) copy-start(f32[8,2]{0,1:T(2,128)} %param.26) | copy-start | bytes 196
  7.2 5.0 %copy-start.8 = (f32[8]{0:T(128)S(1)}, f32[8]{0:T(128)}, u32[]{:S(2)}) copy-start(f32[8]{0:T(128)} %param.23) | copy-start | bytes 100
  7.2 69.3 %copy-start.4 = (f32[8,2,256]{2,1,0:T(2,128)S(1)}, f32[8,2,256]{2,1,0:T(2,128)}, u32[]{:S(2)}) copy-start(f32[8,2,256]{2,1,0:T(2,128)} %param.25) | copy-start | bytes 49156
  7.2 68.2 %reduce-scatter.2.cloned.1.call-start = ((), (), s32[]{:S(2)}) async-start(), calls=%async_computation.1 | async-start | bytes 884736 | tf_op jit(solution)/shard_map/reduce_scatter | solution.py:50
  10.9 144.5 %all-reduce.7.cloned.1.call-start = ((), (), s32[]{:S(2)}) async-start(), calls=%async_computation.2 | async-start | bytes 262144 | tf_op jit(solution)/shard_map/psum | solution.py:87
  82.0 3.4 %copy-start.1 = (f32[8,2,512,256]{3,2,1,0:T(8,128)}, f32[8,2,512,256]{3,2,1,0:T(8,128)S(1)}, u32[]{:S(2)}) copy-start(f32[8,2,512,256]{3,2,1,0:T(8,128)S(1)} %multiply_add_fusion) | copy-start | bytes 25165828
  82.0 34.9 %copy-start.2 = (bf16[1024,512]{1,0:T(8,128)(2,1)S(1)}, bf16[1024,512]{1,0:T(8,128)(2,1)}, u32[]{:S(2)}) copy-start(bf16[1024,512]{1,0:T(8,128)(2,1)} %param.27) | copy-start | bytes 3145732
  82.0 74.4 %copy-start.5 = (f32[512]{0:T(512)S(1)}, f32[512]{0:T(512)}, u32[]{:S(2)}) copy-start(f32[512]{0:T(512)} %param.28) | copy-start | bytes 6148
  117.8 132.8 %all-reduce.11.cloned.1.call-start = ((), (), s32[]{:S(2)}) async-start(), calls=%async_computation.4 | async-start | bytes 2883584 | tf_op jit(solution)/shard_map/psum | solution.py:96
  162.0 121.7 %all-reduce.9.cloned.1.call-start = ((), (), s32[]{:S(2)}) async-start(), calls=%async_computation.3 | async-start | bytes 262144 | tf_op jit(solution)/shard_map/psum | solution.py:102
Sparse Core Ops, SparseCore 0:
  11.9 63.4 reduce-scatter.1
  117.9 37.4 all-reduce.6
  162.1 88.4 all-reduce.10
  254.3 29.3 all-reduce.8
where the time goes:
time: 294 us; the launch traced here: 292 us
  waiting for transfers between devices  167 us (57%)
  blocking collectives  74.3 us (25%)
  matrix products  21.5 us (7%)
  between operations  14.6 us (5%)
  other arithmetic  9.5 us (3%)
  local copies, waits for them, and re-layouts  5 us (2%)
    psum x1, waiting for transfers between devices, per_device(): summed_two = lax.psum((gate_ff, up_ff) + extra_two, 'kv')  70 us
    psum x1, waiting for transfers between devices, per_device(): attn_mix = lax.psum(attn_part, 'tp')  37.5 us
    psum x1, blocking collectives, per_device(): total_one = lax.psum(squares_one, 'kv')  31.5 us
    reduce_scatter x1, waiting for transfers between devices, per_device(): lax.psum_scatter((proj_part, gate_part) + extra_one, 'kv', scatter_dimens...  30.2 us
    psum x1, waiting for transfers between devices, per_device(): down_sum = lax.psum(down_part, 'tp')  28.8 us
    all_gather x1, blocking collectives, per_device(): lax.all_gather(head_out, 'kv', axis=0, tiled=True)  24.2 us
    psum x1, blocking collectives, per_device(): total_two = lax.psum(squares_two, 'kv')  18.6 us
    dot_general x1, matrix products, per_device(): jnp.einsum('bhvd,bhd->bhv', new_c, query, precision=lax.Precision.HIGHEST)  7.17 us
  transfers between devices with their start and end apart: 4, of which 4 were waited for; matrix products, arithmetic and copies ran while one was open for 1% of the time, Pallas kernels for 0%

commit v1 on v0

v1 whole, which is shorter than its diff:
```python
import jax
import jax.numpy as jnp
from jax import lax
from jax.experimental import pallas as pl
from jax.experimental.pallas import tpu as pltpu
from jax.sharding import PartitionSpec as P

norm_floor = 1e-05
MESH = pl.DeviceIdType.MESH
LANES = 128
CHUNK = 512
VMEM_SPEC = pl.BlockSpec(memory_space=pltpu.VMEM)
HBM_SPEC = pl.BlockSpec(memory_space=pltpu.HBM)


def pieces(total):
    return [(at, min(CHUNK, total - at)) for at in range(0, total, CHUNK)]


def peer_of(axis, step):
    count = lax.axis_size(axis)
    return lax.rem(lax.axis_index(axis) + step, count)


def signal_peers(barrier, axis):
    for step in range(1, lax.axis_size(axis)):
        pl.semaphore_signal(
            barrier, inc=1, device_id={axis: peer_of(axis, step)}, device_id_type=MESH
        )


def remote(axis, step, src, dst, send_sem, recv_sem):
    return pltpu.make_async_remote_copy(
        src_ref=src,
        dst_ref=dst,
        send_sem=send_sem,
        recv_sem=recv_sem,
        device_id={axis: peer_of(axis, step)},
        device_id_type=MESH,
    )


def project_kernel(
    tok_ref, gain_ref, wq, wk, wv, wo, wg,
    proj_ref, gate_ref,
    wq_v, wk_v, wv_v, wo_v, wg_v, part, land, gpart, gland,
    load_sem, send_sem, recv_sem, gsend_sem, grecv_sem,
):
    kv = lax.axis_index("kv")
    count = lax.axis_size("kv")
    batch, width = tok_ref.shape
    rows = batch // count
    weights = [(wq, wq_v), (wk, wk_v), (wv, wv_v), (wo, wo_v)]
    loads = [
        pltpu.make_async_copy(wg.at[:, pl.ds(pl.multiple_of(kv * width, LANES), width)], wg_v, load_sem.at[len(weights)])
    ]
    loads += [
        pltpu.make_async_copy(src, dst, load_sem.at[i]) for i, (src, dst) in enumerate(weights)
    ]
    for load in loads:
        load.start()
    barrier = pltpu.get_barrier_semaphore()
    signal_peers(barrier, "kv")
    tok = tok_ref[...].astype(jnp.float32)
    squares = jnp.sum(tok * tok, axis=1, keepdims=True)
    normed = (tok * gain_ref[...]).astype(jnp.bfloat16)
    loads[0].wait()
    gates = lax.dot_general(
        normed, wg_v[...], (((1,), (1,)), ((), ())), preferred_element_type=jnp.float32
    )
    gate_cols = gates.shape[1]
    gpart[...] = jnp.broadcast_to(squares, (batch, LANES)).reshape(count, rows, LANES)
    gpart[:, :, :gate_cols] = gates.reshape(count, rows, gate_cols)
    pl.semaphore_wait(barrier, count - 1)
    copies = []
    for step in range(1, count):
        copy = remote(
            "kv", step, gpart.at[peer_of("kv", step)], gland.at[step],
            gsend_sem.at[step], grecv_sem.at[step],
        )
        copy.start()
        copies.append(copy)
    at = 0
    spans = []
    for i, (_, dst) in enumerate(weights):
        loads[i + 1].wait()
        wide = dst.shape[1]
        for off, size in pieces(wide):
            out = jnp.dot(normed, dst[:, off : off + size], preferred_element_type=jnp.float32)
            part[:, :, at + off : at + off + size] = out.reshape(count, rows, size).astype(
                jnp.bfloat16
            )
        span = pl.ds(at, wide)
        group = []
        for step in range(1, count):
            copy = remote(
                "kv", step, part.at[peer_of("kv", step), :, span], land.at[step, :, span],
                send_sem.at[i, step], recv_sem.at[i, step],
            )
            copy.start()
            group.append(copy)
        spans.append((at, wide, group))
        at += wide
    total = gpart[kv]
    for copy in copies:
        copy.wait_recv()
    for step in range(1, count):
        total += gland[step]
    mean = total[:, gate_cols : gate_cols + 1] / (width * count)
    scale = lax.rsqrt(mean + norm_floor)
    gate_ref[...] = total * scale
    for at, wide, group in spans:
        for copy in group:
            copy.wait_recv()
        acc = part[kv, :, at : at + wide].astype(jnp.float32)
        for step in range(1, count):
            acc += land[step, :, at : at + wide].astype(jnp.float32)
        proj_ref[:, at : at + wide] = acc * scale
    for copy in copies:
        copy.wait_send()
    for _, _, group in spans:
        for copy in group:
            copy.wait_send()


def state_kernel(
    proj_ref, gate_ref, bias_ref, m_ref, n_ref, c_hbm,
    head_ref, newn_ref, newm_ref, newc_hbm,
    held, in_sem, out_sem,
):
    rows, heads, value_size, query_size = held.shape
    tp = lax.axis_index("tp")
    heads_all = bias_ref.shape[1]
    slots = [(h, b) for h in range(heads) for b in range(rows)]
    loads = [
        pltpu.make_async_copy(c_hbm.at[b, h], held.at[b, h], in_sem.at[b, h]) for h, b in slots
    ]
    for load in loads:
        load.start()
    gates = gate_ref[...]
    lane = lax.broadcasted_iota(jnp.int32, gates.shape, 1)
    bias_lane = lax.broadcasted_iota(jnp.int32, bias_ref.shape, 1)
    sub = lax.broadcasted_iota(jnp.int32, (rows, value_size), 0)
    query_width = heads * query_size
    value_at = 2 * query_width
    out_at = value_at + heads * value_size
    stores = []
    for h in range(heads):
        column = tp * heads + h
        log_input = jnp.sum(jnp.where(lane == column, gates, 0.0), axis=1, keepdims=True)
        forget = jnp.sum(jnp.where(lane == heads_all + column, gates, 0.0), axis=1, keepdims=True)
        bias = jnp.sum(jnp.where(bias_lane == column, bias_ref[...], 0.0), axis=1, keepdims=True)
        pre = forget + bias
        log_forget = jnp.minimum(pre, 0.0) - jnp.log(1.0 + jnp.exp(-jnp.abs(pre)))
        carried = log_forget + m_ref[:, h : h + 1]
        new_m = jnp.maximum(carried, log_input)
        keep = jnp.exp(carried - new_m)
        admit = jnp.exp(log_input - new_m)
        newm_ref[:, h : h + 1] = new_m
        query = proj_ref[:, h * query_size : (h + 1) * query_size] * query_size ** (-0.5)
        key_at = query_width + h * query_size
        key = admit * proj_ref[:, key_at : key_at + query_size]
        v_at = value_at + h * value_size
        value = proj_ref[:, v_at : v_at + value_size]
        o_at = out_at + h * value_size
        out_pre = proj_ref[:, o_at : o_at + value_size]
        new_n = keep * n_ref[:, h, :] + key
        newn_ref[:, h, :] = new_n
        value_cols = value.T
        keep_wide = jnp.broadcast_to(keep, (rows, query_size))
        query_low = query.astype(jnp.bfloat16)
        read = jnp.zeros((rows, value_size), jnp.float32)
        for b in range(rows):
            i = h * rows + b
            loads[i].wait()
            old = held[b, h]
            one = lax.dot_general(
                query_low, old.astype(jnp.bfloat16), (((1,), (1,)), ((), ())),
                preferred_element_type=jnp.float32,
            )
            read = jnp.where(sub == b, one, read)
            held[b, h] = (
                keep_wide[b : b + 1, :] * old + value_cols[:, b : b + 1] * key[b : b + 1, :]
            )
            store = pltpu.make_async_copy(held.at[b, h], newc_hbm.at[b, h], out_sem.at[b, h])
            store.start()
            stores.append(store)
        numer = keep * read + value * jnp.sum(key * query, axis=1, keepdims=True)
        denom = jnp.maximum(
            jnp.abs(jnp.sum(new_n * query, axis=1, keepdims=True)), jnp.exp(-new_m)
        )
        gated = numer / ((1.0 + jnp.exp(-out_pre)) * denom)
        head_ref[:, h * value_size : (h + 1) * value_size] = gated.astype(jnp.bfloat16)
    for store in stores:
        store.wait()


def tp_total(buf, send_sem, recv_sem):
    tp = lax.axis_index("tp")
    count = lax.axis_size("tp")
    copies = []
    for step in range(1, count):
        copy = remote("tp", step, buf.at[tp], buf.at[tp], send_sem.at[step], recv_sem.at[step])
        copy.start()
        copies.append(copy)
    for copy in copies:
        copy.wait_recv()
    total = buf[0].astype(jnp.float32)
    for i in range(1, count):
        total += buf[i].astype(jnp.float32)
    return total, copies


def rest_kernel(
    head_ref, tok_ref, gain_ref, wo, wg, wu, wd,
    mixed_ref,
    wo_v, wg_v, wu_v, wd_v, heads_all, abuf, dbuf, gpart, gland, upart, uland, spart, sland, hbuf,
    load_sem, hsend, hrecv, asend, arecv, dsend, drecv, esend, erecv, bsend, brecv,
):
    kv = lax.axis_index("kv")
    tp = lax.axis_index("tp")
    count = lax.axis_size("kv")
    batch, width = tok_ref.shape
    rows = batch // count
    loads = [
        pltpu.make_async_copy(src, dst, load_sem.at[i])
        for i, (src, dst) in enumerate([(wo, wo_v), (wg, wg_v), (wu, wu_v), (wd, wd_v)])
    ]
    barrier = pltpu.get_barrier_semaphore()
    signal_peers(barrier, "kv")
    signal_peers(barrier, "tp")
    for load in loads:
        load.start()
    pl.semaphore_wait(barrier, count - 1 + lax.axis_size("tp") - 1)
    gone = []
    arrive = []
    for step in range(1, count):
        copy = remote(
            "kv", step, head_ref, heads_all.at[kv], hsend.at[step], hrecv.at[step]
        )
        copy.start()
        arrive.append(copy)
    gone += arrive
    heads_all[kv] = head_ref[...]
    loads[0].wait()
    for copy in arrive:
        copy.wait_recv()
    heads = heads_all[...].astype(jnp.float32).reshape(batch, -1).astype(jnp.bfloat16)
    abuf[tp] = jnp.dot(heads, wo_v[...], preferred_element_type=jnp.float32).astype(jnp.bfloat16)
    attn_mix, copies = tp_total(abuf, asend, arecv)
    gone += copies
    middle = (tok_ref[...].astype(jnp.float32) + attn_mix).astype(jnp.bfloat16)
    mid = middle.astype(jnp.float32)
    squares = jnp.sum(mid * mid, axis=1, keepdims=True)
    normed = (mid * gain_ref[...]).astype(jnp.bfloat16)
    spart[...] = jnp.broadcast_to(squares, (batch, LANES)).reshape(count, rows, LANES)
    groups = []
    for i, (weight, part, land) in enumerate(
        [(None, spart, sland), (wg_v, gpart, gland), (wu_v, upart, uland)]
    ):
        if weight is not None:
            loads[i].wait()
            for off, size in pieces(weight.shape[0]):
                out = lax.dot_general(
                    normed, weight[off : off + size, :], (((1,), (1,)), ((), ())),
                    preferred_element_type=jnp.float32,
                )
                part[:, :, off : off + size] = out.reshape(count, rows, size).astype(jnp.bfloat16)
        group = []
        for step in range(1, count):
            copy = remote(
                "kv", step, part.at[peer_of("kv", step)], land.at[step],
                esend.at[i, step], erecv.at[i, step],
            )
            copy.start()
            group.append(copy)
        groups.append((part, land, group))
        gone += group
    sums = []
    for part, land, group in groups:
        for copy in group:
            copy.wait_recv()
        acc = part[kv].astype(jnp.float32)
        for step in range(1, count):
            acc += land[step].astype(jnp.float32)
        sums.append(acc)
    scale = lax.rsqrt(sums[0][:, :1] / (width * count) + norm_floor)
    gate = sums[1] * scale
    hidden = gate / (1.0 + jnp.exp(-gate)) * (sums[2] * scale)
    hbuf[kv] = hidden.astype(jnp.bfloat16)
    arrive = []
    for step in range(1, count):
        copy = remote("kv", step, hbuf.at[kv], hbuf.at[kv], bsend.at[step], brecv.at[step])
        copy.start()
        arrive.append(copy)
    gone += arrive
    loads[3].wait()
    for copy in arrive:
        copy.wait_recv()
    hid = hbuf[...].astype(jnp.float32).reshape(batch, -1).astype(jnp.bfloat16)
    dbuf[tp] = jnp.dot(hid, wd_v[...], preferred_element_type=jnp.float32).astype(jnp.bfloat16)
    down, copies = tp_total(dbuf, dsend, drecv)
    gone += copies
    mixed_ref[...] = (mid + down).astype(jnp.bfloat16)
    for copy in gone:
        copy.wait_send()


def per_device(
    tokens,
    attn_gain,
    w_query,
    w_key,
    w_value,
    w_outgate,
    w_gates,
    forget_bias,
    state_c,
    state_n,
    state_m,
    w_output,
    mlp_gain,
    w_gateff,
    w_upff,
    w_downff,
):
    f32, bf16 = jnp.float32, jnp.bfloat16
    count = lax.axis_size("kv")
    tps = lax.axis_size("tp")
    batch, width = tokens.shape
    rows, heads_dev, value_size, query_size = state_c.shape
    projections = (w_query, w_key, w_value, w_outgate)
    proj_width = sum(w.shape[1] for w in projections)
    hidden = w_gateff.shape[1]
    value_width = heads_dev * value_size
    rest_weights = (w_output, w_gateff.T, w_upff.T, w_downff)
    sem = pltpu.SemaphoreType.DMA
    struct = jax.ShapeDtypeStruct

    proj, gates = pl.pallas_call(
        project_kernel,
        out_shape=(struct((rows, proj_width), f32), struct((rows, LANES), f32)),
        in_specs=[VMEM_SPEC] * 2 + [HBM_SPEC] * 5,
        out_specs=(VMEM_SPEC, VMEM_SPEC),
        scratch_shapes=[pltpu.VMEM(w.shape, bf16) for w in projections]
        + [
            pltpu.VMEM((w_gates.shape[1], width), bf16),
            pltpu.VMEM((count, rows, proj_width), bf16),
            pltpu.VMEM((count, rows, proj_width), bf16),
            pltpu.VMEM((count, rows, LANES), f32),
            pltpu.VMEM((count, rows, LANES), f32),
            sem((5,)),
            sem((4, count)),
            sem((4, count)),
            sem((count,)),
            sem((count,)),
        ],
        compiler_params=pltpu.CompilerParams(
            collective_id=0, has_side_effects=True, vmem_limit_bytes=12 * 2**20
        ),
        name="project",
    )(tokens, attn_gain[None], w_query, w_key, w_value, w_outgate, w_gates.T)

    head_out, new_n, new_m, new_c = pl.pallas_call(
        state_kernel,
        out_shape=(
            struct((rows, value_width), bf16),
            struct(state_n.shape, f32),
            struct(state_m.shape, f32),
            struct(state_c.shape, f32),
        ),
        in_specs=[VMEM_SPEC] * 5 + [HBM_SPEC],
        out_specs=(VMEM_SPEC, VMEM_SPEC, VMEM_SPEC, HBM_SPEC),
        scratch_shapes=[
            pltpu.VMEM(state_c.shape, f32),
            sem((rows, heads_dev)),
            sem((rows, heads_dev)),
        ],
        compiler_params=pltpu.CompilerParams(vmem_limit_bytes=16 * 2**20),
        name="state",
    )(proj, gates, forget_bias[None], state_m, state_n, state_c)

    mixed = pl.pallas_call(
        rest_kernel,
        out_shape=struct((batch, width), bf16),
        in_specs=[VMEM_SPEC] * 3 + [HBM_SPEC] * 4,
        out_specs=VMEM_SPEC,
        scratch_shapes=[pltpu.VMEM(w.shape, bf16) for w in rest_weights]
        + [
            pltpu.VMEM((count, rows, value_width), bf16),
            pltpu.VMEM((tps, batch, width), bf16),
            pltpu.VMEM((tps, batch, width), bf16),
            pltpu.VMEM((count, rows, hidden), bf16),
            pltpu.VMEM((count, rows, hidden), bf16),
            pltpu.VMEM((count, rows, hidden), bf16),
            pltpu.VMEM((count, rows, hidden), bf16),
            pltpu.VMEM((count, rows, LANES), f32),
            pltpu.VMEM((count, rows, LANES), f32),
            pltpu.VMEM((count, rows, hidden), bf16),
            sem((4,)),
            sem((count,)),
            sem((count,)),
            sem((tps,)),
            sem((tps,)),
            sem((tps,)),
            sem((tps,)),
            sem((3, count)),
            sem((3, count)),
            sem((count,)),
            sem((count,)),
        ],
        compiler_params=pltpu.CompilerParams(
            collective_id=1, has_side_effects=True, vmem_limit_bytes=32 * 2**20
        ),
        name="rest",
    )(head_out, tokens, mlp_gain[None], *rest_weights)
    return (mixed, new_c, new_n, new_m)


def solution(mesh):
    placed = (
        P(None, "kv"),
        P("kv"),
        P("kv", "tp"),
        P("kv", "tp"),
        P("kv", "tp"),
        P("kv", "tp"),
        P(),
        P(),
        P("kv", "tp", None, None),
        P("kv", "tp", None),
        P("kv", "tp"),
        P("tp", "kv"),
        P("kv"),
        P("kv", "tp"),
        P("kv", "tp"),
        P("tp", "kv"),
    )
    return jax.shard_map(
        per_device,
        mesh=mesh,
        in_specs=placed,
        out_specs=(P(None, "kv"), P("kv", "tp", None, None), P("kv", "tp", None), P("kv", "tp")),
        check_vma=False,
    )
```

time: 294 us -> 84.1 us (0.29)
  the two profiles are of different devices: /device:TPU:1 before, /device:TPU:27 now
where the time goes in v1:
time: 84.1 us; the launch traced here: 83.5 us
  Pallas kernels  65.6 us (78%)
  local copies, waits for them, and re-layouts  17.2 us (20%)
    pallas_call x1, Pallas kernels, per_device(): pl.pallas_call(rest_kernel, out_shape=struct((batch, width), bf16), in_sp...  47.2 us
    unnamed x35, local copies, waits for them, and re-layouts  17.2 us
    pallas_call x1, Pallas kernels, per_device(): pl.pallas_call(project_kernel, out_shape=(struct((rows, proj_width), f32)...  12.7 us
    pallas_call x1, Pallas kernels, per_device(): pl.pallas_call(state_kernel, out_shape=(struct((rows, value_width), bf16)...  5.66 us

profile of v1, /device:TPU:27, one launch (start us, length us, event | category | flops | bytes accessed | tf_op | source)
XLA Modules:
  0.0 83.5 jit_solution(12359632223601031925)
XLA Ops:
  0.6 0.0 copy-start.12
  0.6 0.8 copy.20.m_ref
  1.4 0.0 copy-start.4
  1.4 1.2 %copy-done.4 = bf16[512,1024]{1,0:T(8,128)(2,1)S(1)} copy-done((bf16[512,1024]{1,0:T(8,128)(2,1)S(1)}, bf16[512,1024]{1,0:T(8,128)(2,1)}, u32[]{:S(2)}) %copy-start.4) | copy-done | bytes 1048600
  2.6 0.0 copy-start.5
  2.6 1.2 %copy-done.5 = bf16[512,1024]{1,0:T(8,128)(2,1)S(1)} copy-done((bf16[512,1024]{1,0:T(8,128)(2,1)S(1)}, bf16[512,1024]{1,0:T(8,128)(2,1)}, u32[]{:S(2)}) %copy-start.5) | copy-done | bytes 1048600
  3.9 0.0 copy-start.7
  3.9 1.0 %copy-done.7 = bf16[512,512]{1,0:T(8,128)(2,1)S(1)} copy-done((bf16[512,512]{1,0:T(8,128)(2,1)S(1)}, bf16[512,512]{1,0:T(8,128)(2,1)}, u32[]{:S(2)}) %copy-start.7) | copy-done | bytes 524312
  4.9 0.0 copy-start.8
  4.9 1.0 %copy-done.8 = bf16[512,512]{1,0:T(8,128)(2,1)S(1)} copy-done((bf16[512,512]{1,0:T(8,128)(2,1)S(1)}, bf16[512,512]{1,0:T(8,128)(2,1)}, u32[]{:S(2)}) %copy-start.8) | copy-done | bytes 524312
  5.9 0.0 copy-start.9
  5.9 0.8 %copy-done.9 = bf16[64,512]{1,0:T(8,128)(2,1)S(1)} copy-done((bf16[64,512]{1,0:T(8,128)(2,1)S(1)}, bf16[64,512]{1,0:T(8,128)(2,1)}, u32[]{:S(2)}) %copy-start.9) | copy-done | bytes 65560
  6.8 0.0 copy-start.11
  6.8 0.9 %copy-done.11 = bf16[4096,16]{0,1:T(8,128)(2,1)S(1)} copy-done((bf16[4096,16]{0,1:T(8,128)(2,1)S(1)}, bf16[4096,16]{0,1:T(8,128)(2,1)}, u32[]{:S(2)}) %copy-start.11) | copy-done | bytes 131096
  7.7 0.0 copy-start.13
  7.7 0.7 copy-done.13
  8.4 0.0 copy-start.15
  8.4 12.7 %project.1 = (f32[8,3072]{1,0:T(8,128)S(1)}, f32[8,128]{1,0:T(8,128)S(1)}) custom-call(bf16[64,512]{1,0:T(8,128)(2,1)S(1)} %copy-done.9, f32[1,512]{1,0:T(1,128)S(1)} %bitcast.9, bf16[512,512]{1,0:T(8,128)(2,1)S(1)} %copy-done.7, bf16[512,512]{1,0:T(8,128)(2,1)S(1)} %copy-done.8, bf16[512,1024]{1,0:T(8,128)(2,1)S(1)} %copy-done.4, ...), custom_call_target="tpu_custom_call" | custom-call | tf_op jit(solution)/shard_map/project/pallas_call | solution.py:340
  21.1 0.0 copy-done.12
  21.1 0.0 copy-done.15
  21.1 0.0 copy-start
  21.1 3.4 %copy-done = f32[8,2,512,256]{3,2,1,0:T(8,128)S(1)} copy-done((f32[8,2,512,256]{3,2,1,0:T(8,128)S(1)}, f32[8,2,512,256]{3,2,1,0:T(8,128)}, u32[]{:S(2)}) %copy-start) | copy-done | bytes 8388632
  24.5 0.0 copy-start.1
  24.5 0.0 copy-start.10
  24.5 0.0 copy-start.14
  24.5 5.7 %state.1 = (bf16[8,1024]{1,0:T(8,128)(2,1)S(1)}, f32[8,2,256]{2,1,0:T(2,128)}, f32[8,2]{1,0:T(8,128)S(1)}, f32[8,2,512,256]{3,2,1,0:T(8,128)}) custom-call(f32[8,3072]{1,0:T(8,128)S(1)} %get-tuple-element.10.proj_ref, f32[8,128]{1,0:T(8,128)S(1)} %get-tuple-element.11.gate_ref, f32[1,8]{1,0:T(1,128)S(1)} %bitcast.11, f32[8,2]{1,0:T(8,128)S(1)} %copy.20.m_ref, ...), custom_call_target="tpu_custom_call" | custom-call | tf_op jit(solution)/shard_map/state/pallas_call | solution.py:364
  30.2 0.6 copy.21
  30.8 0.0 copy-done.1
  30.8 0.0 copy-done.10
  30.8 0.0 copy-done.14
  30.8 0.0 copy-start.2
  30.8 1.8 %copy-done.2 = bf16[512,2752]{0,1:T(8,128)(2,1)S(1)} copy-done((bf16[512,2752]{0,1:T(8,128)(2,1)S(1)}, bf16[512,2752]{0,1:T(8,128)(2,1)}, u32[]{:S(2)}) %copy-start.2) | copy-done | bytes 2818072
  32.6 0.0 copy-start.3
  32.6 1.8 %copy-done.3 = bf16[2752,512]{1,0:T(8,128)(2,1)S(1)} copy-done((bf16[2752,512]{1,0:T(8,128)(2,1)S(1)}, bf16[2752,512]{1,0:T(8,128)(2,1)}, u32[]{:S(2)}) %copy-start.3) | copy-done | bytes 2818072
  34.4 0.0 copy-start.6
  34.4 1.2 %copy-done.6 = bf16[1024,512]{1,0:T(8,128)(2,1)S(1)} copy-done((bf16[1024,512]{1,0:T(8,128)(2,1)S(1)}, bf16[1024,512]{1,0:T(8,128)(2,1)}, u32[]{:S(2)}) %copy-start.6) | copy-done | bytes 1048600
  35.6 47.2 %rest.1 = bf16[64,512]{1,0:T(8,128)(2,1)S(1)} custom-call(bf16[8,1024]{1,0:T(8,128)(2,1)S(1)} %get-tuple-element.12.head_ref, bf16[64,512]{1,0:T(8,128)(2,1)S(1)} %copy-done.10, f32[1,512]{1,0:T(1,128)S(1)} %bitcast.10, bf16[1024,512]{1,0:T(8,128)(2,1)S(1)} %copy-done.6, bf16[2752,512]{1,0:T(8,128)(2,1)S(1)} %bitcast.6, bf16[2752,512]{1,0:T(8,128)(2,1)S(1)} %bitcast.7, ...), custom_call_target="tpu_custom_call" | custom-call | tf_op jit(solution)/shard_map/rest/pallas_call | solution.py:383
  82.9 0.6 copy.23
Async XLA Ops:
  0.6 20.5 %copy-start.12 = (f32[8,2,256]{2,1,0:T(2,128)S(1)}, f32[8,2,256]{2,1,0:T(2,128)}, u32[]{:S(2)}) copy-start(f32[8,2,256]{2,1,0:T(2,128)} %n_ref.1) | copy-start | bytes 49156
  1.4 1.2 %copy-start.4 = (bf16[512,1024]{1,0:T(8,128)(2,1)S(1)}, bf16[512,1024]{1,0:T(8,128)(2,1)}, u32[]{:S(2)}) copy-start(bf16[512,1024]{1,0:T(8,128)(2,1)} %wv.1) | copy-start | bytes 3145732
  2.6 1.2 %copy-start.5 = (bf16[512,1024]{1,0:T(8,128)(2,1)S(1)}, bf16[512,1024]{1,0:T(8,128)(2,1)}, u32[]{:S(2)}) copy-start(bf16[512,1024]{1,0:T(8,128)(2,1)} %wo.2) | copy-start | bytes 3145732
  3.9 1.0 %copy-start.7 = (bf16[512,512]{1,0:T(8,128)(2,1)S(1)}, bf16[512,512]{1,0:T(8,128)(2,1)}, u32[]{:S(2)}) copy-start(bf16[512,512]{1,0:T(8,128)(2,1)} %wq.1) | copy-start | bytes 1572868
  4.9 1.0 %copy-start.8 = (bf16[512,512]{1,0:T(8,128)(2,1)S(1)}, bf16[512,512]{1,0:T(8,128)(2,1)}, u32[]{:S(2)}) copy-start(bf16[512,512]{1,0:T(8,128)(2,1)} %wk.1) | copy-start | bytes 1572868
  5.9 0.8 %copy-start.9 = (bf16[64,512]{1,0:T(8,128)(2,1)S(1)}, bf16[64,512]{1,0:T(8,128)(2,1)}, u32[]{:S(2)}) copy-start(bf16[64,512]{1,0:T(8,128)(2,1)} %tok_ref.3) | copy-start | bytes 196612
  6.8 0.9 %copy-start.11 = (bf16[4096,16]{0,1:T(8,128)(2,1)S(1)}, bf16[4096,16]{0,1:T(8,128)(2,1)}, u32[]{:S(2)}) copy-start(bf16[4096,16]{0,1:T(8,128)(2,1)} %param.22) | copy-start | bytes 393220
  7.7 0.7 copy-start.13
  8.4 12.7 %copy-start.15 = (f32[8]{0:T(128)S(1)}, f32[8]{0:T(128)}, u32[]{:S(2)}) copy-start(f32[8]{0:T(128)} %param.23) | copy-start | bytes 100
  21.1 3.4 %copy-start = (f32[8,2,512,256]{3,2,1,0:T(8,128)S(1)}, f32[8,2,512,256]{3,2,1,0:T(8,128)}, u32[]{:S(2)}) copy-start(f32[8,2,512,256]{3,2,1,0:T(8,128)} %c_hbm.1) | copy-start | bytes 25165828
  24.5 6.3 %copy-start.1 = (bf16[512,2752]{0,1:T(8,128)(2,1)S(1)}, bf16[512,2752]{0,1:T(8,128)(2,1)}, u32[]{:S(2)}) copy-start(bf16[512,2752]{0,1:T(8,128)(2,1)} %param.29) | copy-start | bytes 8454148
  24.5 6.3 %copy-start.10 = (bf16[64,512]{1,0:T(8,128)(2,1)S(1)}, bf16[64,512]{1,0:T(8,128)(2,1)}, u32[]{:S(2)}) copy-start(bf16[64,512]{1,0:T(8,128)(2,1)} %tok_ref.3) | copy-start | bytes 196612
  24.5 6.3 %copy-start.14 = (f32[512]{0:T(512)S(1)}, f32[512]{0:T(512)}, u32[]{:S(2)}) copy-start(f32[512]{0:T(512)} %param.28) | copy-start | bytes 6148
  30.8 1.8 %copy-start.2 = (bf16[512,2752]{0,1:T(8,128)(2,1)S(1)}, bf16[512,2752]{0,1:T(8,128)(2,1)}, u32[]{:S(2)}) copy-start(bf16[512,2752]{0,1:T(8,128)(2,1)} %param.30) | copy-start | bytes 8454148
  32.6 1.8 %copy-start.3 = (bf16[2752,512]{1,0:T(8,128)(2,1)S(1)}, bf16[2752,512]{1,0:T(8,128)(2,1)}, u32[]{:S(2)}) copy-start(bf16[2752,512]{1,0:T(8,128)(2,1)} %wd.1) | copy-start | bytes 8454148
  34.4 1.2 %copy-start.6 = (bf16[1024,512]{1,0:T(8,128)(2,1)S(1)}, bf16[1024,512]{1,0:T(8,128)(2,1)}, u32[]{:S(2)}) copy-start(bf16[1024,512]{1,0:T(8,128)(2,1)} %wo.3) | copy-start | bytes 3145732

commit v2 on v1

--- a/solution.py
+++ b/solution.py
@@ -9,6 +9,9 @@
 MESH = pl.DeviceIdType.MESH
 LANES = 128
 CHUNK = 512
+SPANS = 4
+VMEM_ALL = 67043328
+SLACK = 640 * 1024
 VMEM_SPEC = pl.BlockSpec(memory_space=pltpu.VMEM)
 HBM_SPEC = pl.BlockSpec(memory_space=pltpu.HBM)
 
@@ -40,11 +43,98 @@
     )
 
 
+def inner_size(count):
+    size = 1 << ((count.bit_length() - 1) // 2)
+    return size if count % size == 0 else 1
+
+
+def place():
+    count = lax.axis_size("kv")
+    inner = inner_size(count)
+    kv = lax.axis_index("kv")
+    return kv // inner, kv % inner, count // inner, inner
+
+
+def inner_peer(step):
+    outer_at, inner_at, _, inner = place()
+    return (inner_at + step) % inner, outer_at * inner + (inner_at + step) % inner
+
+
+def outer_peer(step):
+    outer_at, inner_at, outer, inner = place()
+    return (outer_at + step) % outer, ((outer_at + step) % outer) * inner + inner_at
+
+
+def send_to(device, src, dst, send_sem, recv_sem):
+    copy = pltpu.make_async_remote_copy(
+        src_ref=src,
+        dst_ref=dst,
+        send_sem=send_sem,
+        recv_sem=recv_sem,
+        device_id={"kv": device},
+        device_id_type=MESH,
+    )
+    copy.start()
+    return copy
+
+
+def scatter_first(i, part, land, columns, send_sem, recv_sem):
+    _, _, _, inner = place()
+    copies = []
+    for step in range(1, inner):
+        at, device = inner_peer(step)
+        copies.append(
+            send_to(
+                device, part.at[at, :, :, columns], land.at[step, :, :, columns],
+                send_sem.at[i, step], recv_sem.at[i, step],
+            )
+        )
+    return copies
+
+
+def scatter_second(i, first, part, land, both, last, at, size, send_sem, recv_sem):
+    _, inner_at, outer, inner = place()
+    columns = pl.ds(at, size)
+    for copy in first:
+        copy.wait_recv()
+    acc = part[inner_at, :, :, at : at + size].astype(jnp.float32)
+    for step in range(1, inner):
+        acc += land[step, :, :, at : at + size].astype(jnp.float32)
+    both[:, :, at : at + size] = acc.astype(jnp.bfloat16)
+    copies = []
+    for step in range(1, outer):
+        to, device = outer_peer(step)
+        copies.append(
+            send_to(
+                device, both.at[to, :, columns], last.at[step, :, columns],
+                send_sem.at[i, step], recv_sem.at[i, step],
+            )
+        )
+    return copies
+
+
+def scatter_sum(second, both, last, at, size):
+    outer_at, _, outer, _ = place()
+    for copy in second:
+        copy.wait_recv()
+    acc = both[outer_at, :, at : at + size].astype(jnp.float32)
+    for step in range(1, outer):
+        acc += last[step, :, at : at + size].astype(jnp.float32)
+    return acc
+
+
+def put_part(part, out, at, size):
+    inner, outer, rows, _ = part.shape
+    split = out.reshape(outer, inner, rows, size).astype(jnp.bfloat16)
+    for i in range(inner):
+        part[i, :, :, at : at + size] = split[:, i]
+
+
 def project_kernel(
     tok_ref, gain_ref, wq, wk, wv, wo, wg,
     proj_ref, gate_ref,
-    wq_v, wk_v, wv_v, wo_v, wg_v, part, land, gpart, gland,
-    load_sem, send_sem, recv_sem, gsend_sem, grecv_sem,
+    wq_v, wk_v, wv_v, wo_v, wg_v, part, land, both, last, gpart, gland,
+    load_sem, send_sem, recv_sem, send2_sem, recv2_sem, gsend_sem, grecv_sem,
 ):
     kv = lax.axis_index("kv")
     count = lax.axis_size("kv")
@@ -57,10 +147,10 @@
     loads += [
         pltpu.make_async_copy(src, dst, load_sem.at[i]) for i, (src, dst) in enumerate(weights)
     ]
+    barrier = pltpu.get_barrier_semaphore()
+    signal_peers(barrier, "kv")
     for load in loads:
         load.start()
-    barrier = pltpu.get_barrier_semaphore()
-    signal_peers(barrier, "kv")
     tok = tok_ref[...].astype(jnp.float32)
     squares = jnp.sum(tok * tok, axis=1, keepdims=True)
     normed = (tok * gain_ref[...]).astype(jnp.bfloat16)
@@ -81,26 +171,20 @@
         copy.start()
         copies.append(copy)
     at = 0
-    spans = []
+    groups = []
     for i, (_, dst) in enumerate(weights):
         loads[i + 1].wait()
         wide = dst.shape[1]
         for off, size in pieces(wide):
             out = jnp.dot(normed, dst[:, off : off + size], preferred_element_type=jnp.float32)
-            part[:, :, at + off : at + off + size] = out.reshape(count, rows, size).astype(
-                jnp.bfloat16
-            )
-        span = pl.ds(at, wide)
-        group = []
-        for step in range(1, count):
-            copy = remote(
-                "kv", step, part.at[peer_of("kv", step), :, span], land.at[step, :, span],
-                send_sem.at[i, step], recv_sem.at[i, step],
-            )
-            copy.start()
-            group.append(copy)
-        spans.append((at, wide, group))
+            put_part(part, out, at + off, size)
+        copies_one = scatter_first(i, part, land, pl.ds(at, wide), send_sem, recv_sem)
+        groups.append((at, wide, copies_one))
         at += wide
+    seconds = [
+        scatter_second(i, first, part, land, both, last, at, wide, send2_sem, recv2_sem)
+        for i, (at, wide, first) in enumerate(groups)
+    ]
     total = gpart[kv]
     for copy in copies:
         copy.wait_recv()
@@ -109,17 +193,12 @@
     mean = total[:, gate_cols : gate_cols + 1] / (width * count)
     scale = lax.rsqrt(mean + norm_floor)
     gate_ref[...] = total * scale
-    for at, wide, group in spans:
-        for copy in group:
-            copy.wait_recv()
-        acc = part[kv, :, at : at + wide].astype(jnp.float32)
-        for step in range(1, count):
-            acc += land[step, :, at : at + wide].astype(jnp.float32)
-        proj_ref[:, at : at + wide] = acc * scale
+    for (at, wide, _), second in zip(groups, seconds):
+        proj_ref[:, at : at + wide] = scatter_sum(second, both, last, at, wide) * scale
     for copy in copies:
         copy.wait_send()
-    for _, _, group in spans:
-        for copy in group:
+    for (_, _, first), second in zip(groups, seconds):
+        for copy in first + second:
             copy.wait_send()
 
 
@@ -131,9 +210,10 @@
     rows, heads, value_size, query_size = held.shape
     tp = lax.axis_index("tp")
     heads_all = bias_ref.shape[1]
-    slots = [(h, b) for h in range(heads) for b in range(rows)]
     loads = [
-        pltpu.make_async_copy(c_hbm.at[b, h], held.at[b, h], in_sem.at[b, h]) for h, b in slots
+        pltpu.make_async_copy(c_hbm.at[b, h], held.at[b, h], in_sem.at[b, h])
+        for h in range(heads)
+        for b in range(rows)
     ]
     for load in loads:
         load.start()
@@ -171,8 +251,7 @@
         query_low = query.astype(jnp.bfloat16)
         read = jnp.zeros((rows, value_size), jnp.float32)
         for b in range(rows):
-            i = h * rows + b
-            loads[i].wait()
+            loads[h * rows + b].wait()
             old = held[b, h]
             one = lax.dot_general(
                 query_low, old.astype(jnp.bfloat16), (((1,), (1,)), ((), ())),
@@ -195,6 +274,11 @@
         store.wait()
 
 
+def hidden_spans(hidden):
+    wide = -(-hidden // (SPANS * LANES)) * LANES
+    return [(at, min(wide, hidden - at)) for at in range(0, hidden, wide)]
+
+
 def tp_total(buf, send_sem, recv_sem):
     tp = lax.axis_index("tp")
     count = lax.axis_size("tp")
@@ -214,8 +298,10 @@
 def rest_kernel(
     head_ref, tok_ref, gain_ref, wo, wg, wu, wd,
     mixed_ref,
-    wo_v, wg_v, wu_v, wd_v, heads_all, abuf, dbuf, gpart, gland, upart, uland, spart, sland, hbuf,
-    load_sem, hsend, hrecv, asend, arecv, dsend, drecv, esend, erecv, bsend, brecv,
+    wo_v, wg_v, wu_v, wd_v, heads_all, abuf, dbuf, gpart, gland, gboth, glast,
+    upart, uland, uboth, ulast, spart, sland, hbuf,
+    load_sem, hsend, hrecv, asend, arecv, dsend, drecv, ssend, srecv, esend, erecv, fsend, frecv,
+    bsend, brecv, csend, crecv,
 ):
     kv = lax.axis_index("kv")
     tp = lax.axis_index("tp")
@@ -254,46 +340,63 @@
     squares = jnp.sum(mid * mid, axis=1, keepdims=True)
     normed = (mid * gain_ref[...]).astype(jnp.bfloat16)
     spart[...] = jnp.broadcast_to(squares, (batch, LANES)).reshape(count, rows, LANES)
+    square_copies = [
+        send_to(
+            peer_of("kv", step), spart.at[peer_of("kv", step)], sland.at[step],
+            ssend.at[step], srecv.at[step],
+        )
+        for step in range(1, count)
+    ]
+    gone += square_copies
+    hidden = wg_v.shape[0]
+    spans = hidden_spans(hidden)
     groups = []
-    for i, (weight, part, land) in enumerate(
-        [(None, spart, sland), (wg_v, gpart, gland), (wu_v, upart, uland)]
+    for w, (weight, part, land, both, last) in enumerate(
+        [(wg_v, gpart, gland, gboth, glast), (wu_v, upart, uland, uboth, ulast)]
     ):
-        if weight is not None:
-            loads[i].wait()
-            for off, size in pieces(weight.shape[0]):
+        loads[w + 1].wait()
+        for k, (at, wide) in enumerate(spans):
+            for off, size in pieces(wide):
                 out = lax.dot_general(
-                    normed, weight[off : off + size, :], (((1,), (1,)), ((), ())),
+                    normed, weight[at + off : at + off + size, :], (((1,), (1,)), ((), ())),
                     preferred_element_type=jnp.float32,
                 )
-                part[:, :, off : off + size] = out.reshape(count, rows, size).astype(jnp.bfloat16)
-        group = []
-        for step in range(1, count):
-            copy = remote(
-                "kv", step, part.at[peer_of("kv", step)], land.at[step],
-                esend.at[i, step], erecv.at[i, step],
+                put_part(part, out, at + off, size)
+            i = w * len(spans) + k
+            first = scatter_first(i, part, land, pl.ds(at, wide), esend, erecv)
+            groups.append((i, first, part, land, both, last, at, wide))
+            gone += first
+    seconds = [scatter_second(*group, fsend, frecv) for group in groups]
+    for second in seconds:
+        gone += second
+    for copy in square_copies:
+        copy.wait_recv()
+    total = spart[kv]
+    for step in range(1, count):
+        total += sland[step]
+    scale = lax.rsqrt(total[:, :1] / (width * count) + norm_floor)
+    outer_at, inner_at, outer, inner = place()
+    for k, (at, wide) in enumerate(spans):
+        gate = scatter_sum(seconds[k], gboth, glast, at, wide) * scale
+        up = scatter_sum(seconds[k + len(spans)], uboth, ulast, at, wide) * scale
+        hid = gate / (1.0 + jnp.exp(-gate)) * up
+        hbuf[outer_at, inner_at, :, at : at + wide] = hid.astype(jnp.bfloat16)
+    own = hbuf.at[outer_at, inner_at]
+    along = [
+        send_to(outer_peer(step)[1], own, own, bsend.at[step], brecv.at[step])
+        for step in range(1, outer)
+    ]
+    across = []
+    for far in range(outer):
+        if far > 0:
+            along[far - 1].wait_recv()
+        block = hbuf.at[(outer_at + outer - far) % outer, inner_at]
+        for step in range(1, inner):
+            across.append(
+                send_to(inner_peer(step)[1], block, block, csend.at[far, step], crecv.at[far, step])
             )
-            copy.start()
-            group.append(copy)
-        groups.append((part, land, group))
-        gone += group
-    sums = []
-    for part, land, group in groups:
-        for copy in group:
-            copy.wait_recv()
-        acc = part[kv].astype(jnp.float32)
-        for step in range(1, count):
-            acc += land[step].astype(jnp.float32)
-        sums.append(acc)
-    scale = lax.rsqrt(sums[0][:, :1] / (width * count) + norm_floor)
-    gate = sums[1] * scale
-    hidden = gate / (1.0 + jnp.exp(-gate)) * (sums[2] * scale)
-    hbuf[kv] = hidden.astype(jnp.bfloat16)
-    arrive = []
-    for step in range(1, count):
-        copy = remote("kv", step, hbuf.at[kv], hbuf.at[kv], bsend.at[step], brecv.at[step])
-        copy.start()
-        arrive.append(copy)
-    gone += arrive
+    arrive = across
+    gone += along + across
     loads[3].wait()
     for copy in arrive:
         copy.wait_recv()
@@ -334,29 +437,40 @@
     hidden = w_gateff.shape[1]
     value_width = heads_dev * value_size
     rest_weights = (w_output, w_gateff.T, w_upff.T, w_downff)
+    inner = inner_size(count)
+    outer = count // inner
+    spans = len(hidden_spans(hidden))
     sem = pltpu.SemaphoreType.DMA
     struct = jax.ShapeDtypeStruct
 
     proj, gates = pl.pallas_call(
         project_kernel,
-        out_shape=(struct((rows, proj_width), f32), struct((rows, LANES), f32)),
+        out_shape=(
+            struct((rows, proj_width), f32),
+            struct((rows, LANES), f32),
+        ),
         in_specs=[VMEM_SPEC] * 2 + [HBM_SPEC] * 5,
         out_specs=(VMEM_SPEC, VMEM_SPEC),
         scratch_shapes=[pltpu.VMEM(w.shape, bf16) for w in projections]
         + [
             pltpu.VMEM((w_gates.shape[1], width), bf16),
-            pltpu.VMEM((count, rows, proj_width), bf16),
-            pltpu.VMEM((count, rows, proj_width), bf16),
+            pltpu.VMEM((inner, outer, rows, proj_width), bf16),
+            pltpu.VMEM((inner, outer, rows, proj_width), bf16),
+            pltpu.VMEM((outer, rows, proj_width), bf16),
+            pltpu.VMEM((outer, rows, proj_width), bf16),
             pltpu.VMEM((count, rows, LANES), f32),
             pltpu.VMEM((count, rows, LANES), f32),
             sem((5,)),
-            sem((4, count)),
-            sem((4, count)),
+            sem((4, inner)),
+            sem((4, inner)),
+            sem((4, outer)),
+            sem((4, outer)),
             sem((count,)),
             sem((count,)),
         ],
         compiler_params=pltpu.CompilerParams(
-            collective_id=0, has_side_effects=True, vmem_limit_bytes=12 * 2**20
+            collective_id=0, has_side_effects=True,
+            vmem_limit_bytes=VMEM_ALL - SLACK,
         ),
         name="project",
     )(tokens, attn_gain[None], w_query, w_key, w_value, w_outgate, w_gates.T)
@@ -376,7 +490,7 @@
             sem((rows, heads_dev)),
             sem((rows, heads_dev)),
         ],
-        compiler_params=pltpu.CompilerParams(vmem_limit_bytes=16 * 2**20),
+        compiler_params=pltpu.CompilerParams(vmem_limit_bytes=VMEM_ALL - SLACK),
         name="state",
     )(proj, gates, forget_bias[None], state_m, state_n, state_c)
 
@@ -390,13 +504,18 @@
             pltpu.VMEM((count, rows, value_width), bf16),
             pltpu.VMEM((tps, batch, width), bf16),
             pltpu.VMEM((tps, batch, width), bf16),
-            pltpu.VMEM((count, rows, hidden), bf16),
-            pltpu.VMEM((count, rows, hidden), bf16),
-            pltpu.VMEM((count, rows, hidden), bf16),
-            pltpu.VMEM((count, rows, hidden), bf16),
+        ]
+        + [
+            pltpu.VMEM((inner, outer, rows, hidden), bf16),
+            pltpu.VMEM((inner, outer, rows, hidden), bf16),
+            pltpu.VMEM((outer, rows, hidden), bf16),
+            pltpu.VMEM((outer, rows, hidden), bf16),
+        ]
+        * 2
+        + [
             pltpu.VMEM((count, rows, LANES), f32),
             pltpu.VMEM((count, rows, LANES), f32),
-            pltpu.VMEM((count, rows, hidden), bf16),
+            pltpu.VMEM((outer, inner, rows, hidden), bf16),
             sem((4,)),
             sem((count,)),
             sem((count,)),
@@ -404,13 +523,19 @@
             sem((tps,)),
             sem((tps,)),
             sem((tps,)),
-            sem((3, count)),
-            sem((3, count)),
             sem((count,)),
             sem((count,)),
+            sem((2 * spans, inner)),
+            sem((2 * spans, inner)),
+            sem((2 * spans, outer)),
+            sem((2 * spans, outer)),
+            sem((outer,)),
+            sem((outer,)),
+            sem((outer, inner)),
+            sem((outer, inner)),
         ],
         compiler_params=pltpu.CompilerParams(
-            collective_id=1, has_side_effects=True, vmem_limit_bytes=32 * 2**20
+            collective_id=1, has_side_effects=True, vmem_limit_bytes=VMEM_ALL - SLACK
         ),
         name="rest",
     )(head_out, tokens, mlp_gain[None], *rest_weights)

time: 84.1 us -> 71.2 us (0.85)
  the two profiles are of different devices: /device:TPU:27 before, /device:TPU:1 now
where the time goes in v2:
time: 71.2 us; the launch traced here: 70.8 us
  Pallas kernels  66.1 us (93%)
  local copies, waits for them, and re-layouts  4.13 us (6%)
    pallas_call x1, Pallas kernels, per_device(): pl.pallas_call(rest_kernel, out_shape=struct((batch, width), bf16), in_sp...  42.9 us
    pallas_call x1, Pallas kernels, per_device(): pl.pallas_call(project_kernel, out_shape=(struct((rows, proj_width), f32)...  14.9 us
    pallas_call x1, Pallas kernels, per_device(): pl.pallas_call(state_kernel, out_shape=(struct((rows, value_width), bf16)...  8.2 us
    unnamed x3, local copies, waits for them, and re-layouts  4.13 us

profile of v2, /device:TPU:1, one launch (start us, length us, event | category | flops | bytes accessed | tf_op | source)
XLA Modules:
  0.0 70.8 jit_solution(6969760984309565263)
XLA Ops:
  0.6 1.3 %copy.20.m_ref = f32[8,2]{1,0:T(8,128)} copy(f32[8,2]{0,1:T(2,128)} %param.26) | data formatting | bytes 128 | tf_op args[10]
  2.0 14.9 %project.1 = (f32[8,3072]{1,0:T(8,128)}, f32[8,128]{1,0:T(8,128)}) custom-call(bf16[64,512]{1,0:T(8,128)(2,1)} %tok_ref.3, f32[1,512]{1,0:T(1,128)} %bitcast.9, bf16[512,512]{1,0:T(8,128)(2,1)} %wq.1, bf16[512,512]{1,0:T(8,128)(2,1)} %wk.1, bf16[512,1024]{1,0:T(8,128)(2,1)} %wv.1, bf16[512,1024]{1,0:T(8,128)(2,1)} %wo.2, bf16[16,4096]{1,0:T(8,128)(2,1)} %bitcast.8), custom_call_target="tpu_custom_call" | custom-call | tf_op jit(solution)/shard_map/project/pallas_call | solution.py:446
  16.9 8.2 %state.1 = (bf16[8,1024]{1,0:T(8,128)(2,1)}, f32[8,2,256]{2,1,0:T(2,128)}, f32[8,2]{1,0:T(8,128)}, f32[8,2,512,256]{3,2,1,0:T(8,128)}) custom-call(f32[8,3072]{1,0:T(8,128)} %get-tuple-element.10.proj_ref, f32[8,128]{1,0:T(8,128)} %get-tuple-element.11.gate_ref, f32[1,8]{1,0:T(1,128)} %bitcast.11, f32[8,2]{1,0:T(8,128)} %copy.20.m_ref, f32[8,2,256]{2,1,0:T(2,128)} %n_ref.1, ...), custom_call_target="tpu_custom_call" | custom-call | tf_op jit(solution)/shard_map/state/pallas_call | solution.py:478
  25.1 1.3 %copy.21 = f32[8,2]{0,1:T(2,128)} copy(f32[8,2]{1,0:T(8,128)} %get-tuple-element.19) | data formatting | bytes 128
  26.4 42.9 %rest.1 = bf16[64,512]{1,0:T(8,128)(2,1)} custom-call(bf16[8,1024]{1,0:T(8,128)(2,1)} %get-tuple-element.12.head_ref, bf16[64,512]{1,0:T(8,128)(2,1)} %tok_ref.3, f32[1,512]{1,0:T(1,128)} %bitcast.10, bf16[1024,512]{1,0:T(8,128)(2,1)} %wo.3, bf16[2752,512]{1,0:T(8,128)(2,1)} %bitcast.6, bf16[2752,512]{1,0:T(8,128)(2,1)} %bitcast.7, bf16[2752,512]{1,0:T(8,128)(2,1)} %wd.1), custom_call_target="tpu_custom_call" | custom-call | tf_op jit(solution)/shard_map/rest/pallas_call | solution.py:497
  69.4 1.5 %copy.23 = bf16[64,512]{1,0:T(8,128)(2,1)} copy(bf16[64,512]{1,0:T(8,128)(2,1)} %rest.1) | data formatting | bytes 131072

commit v3 on v2

--- a/solution.py
+++ b/solution.py
@@ -221,6 +221,9 @@
     lane = lax.broadcasted_iota(jnp.int32, gates.shape, 1)
     bias_lane = lax.broadcasted_iota(jnp.int32, bias_ref.shape, 1)
     sub = lax.broadcasted_iota(jnp.int32, (rows, value_size), 0)
+    eye = lax.broadcasted_iota(jnp.int32, (rows, rows), 0) == lax.broadcasted_iota(
+        jnp.int32, (rows, rows), 1
+    )
     query_width = heads * query_size
     value_at = 2 * query_width
     out_at = value_at + heads * value_size
@@ -232,11 +235,12 @@
         bias = jnp.sum(jnp.where(bias_lane == column, bias_ref[...], 0.0), axis=1, keepdims=True)
         pre = forget + bias
         log_forget = jnp.minimum(pre, 0.0) - jnp.log(1.0 + jnp.exp(-jnp.abs(pre)))
-        carried = log_forget + m_ref[:, h : h + 1]
+        old_m = jnp.sum(jnp.where(eye, m_ref[h : h + 1, :], 0.0), axis=1, keepdims=True)
+        carried = log_forget + old_m
         new_m = jnp.maximum(carried, log_input)
         keep = jnp.exp(carried - new_m)
         admit = jnp.exp(log_input - new_m)
-        newm_ref[:, h : h + 1] = new_m
+        newm_ref[h : h + 1, :] = jnp.sum(jnp.where(eye, new_m, 0.0), axis=0, keepdims=True)
         query = proj_ref[:, h * query_size : (h + 1) * query_size] * query_size ** (-0.5)
         key_at = query_width + h * query_size
         key = admit * proj_ref[:, key_at : key_at + query_size]
@@ -480,7 +484,7 @@
         out_shape=(
             struct((rows, value_width), bf16),
             struct(state_n.shape, f32),
-            struct(state_m.shape, f32),
+            struct(state_m.T.shape, f32),
             struct(state_c.shape, f32),
         ),
         in_specs=[VMEM_SPEC] * 5 + [HBM_SPEC],
@@ -492,7 +496,7 @@
         ],
         compiler_params=pltpu.CompilerParams(vmem_limit_bytes=VMEM_ALL - SLACK),
         name="state",
-    )(proj, gates, forget_bias[None], state_m, state_n, state_c)
+    )(proj, gates, forget_bias[None], state_m.T, state_n, state_c)
 
     mixed = pl.pallas_call(
         rest_kernel,
@@ -539,7 +543,7 @@
         ),
         name="rest",
     )(head_out, tokens, mlp_gain[None], *rest_weights)
-    return (mixed, new_c, new_n, new_m)
+    return (mixed, new_c, new_n, new_m.T)
 
 
 def solution(mesh):

time: 71.2 us -> 68.5 us (0.962)
  local copies, waits for them, and re-layouts: 4.13 us -> 1.47 us
    unnamed x3 -> x1, local copies, waits for them, and re-layouts: 4.13 us -> 1.47 us
where the time goes in v3:
time: 68.5 us; the launch traced here: 68.2 us
  Pallas kernels  66.1 us (96%)
  local copies, waits for them, and re-layouts  1.47 us (2%)
    pallas_call x1, Pallas kernels, per_device(): pl.pallas_call(rest_kernel, out_shape=struct((batch, width), bf16), in_sp...  42.9 us
    pallas_call x1, Pallas kernels, per_device(): pl.pallas_call(project_kernel, out_shape=(struct((rows, proj_width), f32)...  15 us
    pallas_call x1, Pallas kernels, per_device(): pl.pallas_call(state_kernel, out_shape=(struct((rows, value_width), bf16)...  8.22 us
    unnamed x1, local copies, waits for them, and re-layouts  1.47 us

profile of v3, /device:TPU:1, one launch (start us, length us, event | category | flops | bytes accessed | tf_op | source)
XLA Modules:
  0.0 68.2 jit_solution(4372757698793335108)
XLA Ops:
  0.6 15.0 %project.1 = (f32[8,3072]{1,0:T(8,128)}, f32[8,128]{1,0:T(8,128)}) custom-call(bf16[64,512]{1,0:T(8,128)(2,1)} %tok_ref.3, f32[1,512]{1,0:T(1,128)} %bitcast.11, bf16[512,512]{1,0:T(8,128)(2,1)} %wq.1, bf16[512,512]{1,0:T(8,128)(2,1)} %wk.1, bf16[512,1024]{1,0:T(8,128)(2,1)} %wv.1, bf16[512,1024]{1,0:T(8,128)(2,1)} %wo.2, bf16[16,4096]{1,0:T(8,128)(2,1)} %bitcast.10), custom_call_target="tpu_custom_call" | custom-call | tf_op jit(solution)/shard_map/project/pallas_call | solution.py:450
  15.6 8.2 %state.1 = (bf16[8,1024]{1,0:T(8,128)(2,1)}, f32[8,2,256]{2,1,0:T(2,128)}, f32[2,8]{1,0:T(2,128)}, f32[8,2,512,256]{3,2,1,0:T(8,128)}) custom-call(f32[8,3072]{1,0:T(8,128)} %get-tuple-element.10.proj_ref, f32[8,128]{1,0:T(8,128)} %get-tuple-element.11.gate_ref, f32[1,8]{1,0:T(1,128)} %bitcast.14, f32[2,8]{1,0:T(2,128)} %bitcast.13, f32[8,2,256]{2,1,0:T(2,128)} %n_ref.1, ...), custom_call_target="tpu_custom_call" | custom-call | tf_op jit(solution)/shard_map/state/pallas_call | solution.py:482
  23.8 42.9 %rest.1 = bf16[64,512]{1,0:T(8,128)(2,1)} custom-call(bf16[8,1024]{1,0:T(8,128)(2,1)} %get-tuple-element.12.head_ref, bf16[64,512]{1,0:T(8,128)(2,1)} %tok_ref.3, f32[1,512]{1,0:T(1,128)} %bitcast.12, bf16[1024,512]{1,0:T(8,128)(2,1)} %wo.3, bf16[2752,512]{1,0:T(8,128)(2,1)} %bitcast.8, bf16[2752,512]{1,0:T(8,128)(2,1)} %bitcast.9, bf16[2752,512]{1,0:T(8,128)(2,1)} %wd.1), custom_call_target="tpu_custom_call" | custom-call | tf_op jit(solution)/shard_map/rest/pallas_call | solution.py:501
  66.8 1.5 %copy.21 = bf16[64,512]{1,0:T(8,128)(2,1)} copy(bf16[64,512]{1,0:T(8,128)(2,1)} %rest.1) | data formatting | bytes 131072
